TPU v7x, 512 devices: a whole 4x4x16 slice. The times are simulated.
512 devices in a mesh: kv: 64 (over z, y), tp: 8 (over x, core).
Axes of the slice: x: 4, y: 4, z: 16, core: 2. Of those that a mesh axis runs over, the one named last changes fastest.
Arguments:
- tokens: bfloat16 [32, 4096], P(None, 'kv'), may hold values from -6 to 6
- norm_gain: bfloat16 [4096], P('kv'), may hold values from 0.099609375 to 1.8984375
- w_query: bfloat16 [4096, 4096], P('kv', 'tp'), may hold values from -0.09375 to 0.09375
- w_key: bfloat16 [4096, 1024], P('kv', 'tp'), may hold values from -0.09375 to 0.09375
- w_value: bfloat16 [4096, 1024], P('kv', 'tp'), may hold values from -0.09375 to 0.09375
- w_forget: bfloat16 [4096, 32], P('kv', 'tp'), may hold values from -0.1875 to 0.1875
- forget_bias: float32 [32], P('tp'), may hold values from -1 to 3
- key_cache: bfloat16 [32, 16384, 1024], P(None, 'kv', 'tp'), may hold values from -1200 to 1200
- value_cache: bfloat16 [32, 16384, 1024], P(None, 'kv', 'tp'), may hold values from -6 to 6
- gate_cache: float32 [32, 32, 16384], P(None, 'tp', 'kv'), may hold values from -2051 to 0
- lengths: int32 [32], replicated, may hold values from 4096 to 16383, as said below
- w_out: bfloat16 [4096, 4096], P('tp', 'kv'), may hold values from -0.375 to 0.375
Outputs:
- mixed: bfloat16 [32, 4096], P(None, 'kv')
Inputs may be any that keep to these rules, and one draw needn't show every extreme that they name: `lengths`: at least one sequence has the length 16383 in every draw.
All inputs are finite; a program needn't handle non-finite values.
Results may differ from a plain program's by a relative error of at most 0.018.
Values may be sent and summed in bfloat16 or wider, within the bound.
A program may use at most 64 MiB of HBM per device.

v0:
```python
import jax
import jax.numpy as jnp
from jax import lax
from jax.sharding import Mesh
from jax.sharding import PartitionSpec as P

D = 4096
HEAD_DIM = 128
KV = ("kv_0", "kv_1")


EPSILON = 1e-06
NEGATIVE = -1e30


def filled_up(lines, size):
    spare = -lines.shape[0] % size
    if not spare:
        return lines
    return jnp.concatenate([lines, jnp.zeros((spare, *lines.shape[1:]), lines.dtype)])


def joined_along(tiles, dim):
    tiles = jnp.moveaxis(tiles, 0, dim)
    lengths = tiles.shape
    return tiles.reshape(*lengths[:dim], lengths[dim] * lengths[dim + 1], *lengths[dim + 2 :])


def copy_for_each(x, axis):
    size = lax.axis_size(axis)
    return lax.all_to_all(jnp.broadcast_to(x[None], (size, *x.shape)), axis, 0, 0, tiled=True)


def gather_directly(x, axis, dim):
    return joined_along(copy_for_each(x, axis), dim)


def split_up(x, dim, size):
    before, after = (x.shape[:dim], x.shape[dim + 1 :])
    return jnp.moveaxis(x.reshape(*before, size, -1, *after), dim, 0)


def summed_on_arrival(x, axis, dim):
    tiles = split_up(x, dim, lax.axis_size(axis))
    arrived = lax.all_to_all(tiles, axis, split_axis=0, concat_axis=0, tiled=True)
    return arrived.sum(axis=0)


def sum_by_parts(x, axes):
    padded = filled_up(x, lax.axis_size(axes))
    whole = gather_directly(summed_on_arrival(padded, axes, 0), axes, 0)
    return lax.slice_in_dim(whole, 0, len(x)).reshape(x.shape)


def packed_total(arrays, axis):
    flat, at, finished = (jnp.concatenate([a.reshape(-1) for a in arrays]), 0, [])
    running = sum_by_parts(flat, axis)
    for a in arrays:
        finished.append(running[at : at + a.size].reshape(a.shape))
        at += a.size
    return tuple(finished)


def gathered_once(x, axis):
    leaves = jax.tree.leaves(x)
    turns = sorted(range(len(leaves)), key=lambda k: -leaves[k].size)
    width = (1, *leaves[turns[0]].shape)[-1]
    lines = [
        jnp.pad(leaves[k].reshape(-1), (0, -leaves[k].size % width)).reshape(-1, width)
        for k in turns
    ]
    both, at, found = (lax.all_gather(jnp.concatenate(lines), axis), 0, {})
    for k, line in zip(turns, lines):
        piece = both[:, at : at + len(line)].reshape(len(both), -1)
        found[k] = piece[:, : leaves[k].size].reshape(-1, *leaves[k].shape)
        at += len(line)
    numbers = iter(range(len(leaves)))
    return jax.tree.map(lambda _: found[next(numbers)], x)


def merged_by_axis(x, axes, combine):
    for axis in axes:
        pieces = gathered_once(x, axis)
        x = jax.tree.map(lambda part: part[0], pieces)
        for k in range(1, lax.axis_size(axis)):
            x = combine(x, jax.tree.map(lambda part: part[k], pieces))
    return x


def over_copies(x, axis):
    return copy_for_each(x, axis).astype(jnp.float32).sum(axis=0)


def combine_parts(earlier, later):
    top_a, total_a, weighted_a = earlier
    top_b, total_b, weighted_b = later
    highest = jnp.maximum(top_a, top_b)
    factor_a = jnp.exp(top_a - highest)
    factor_b = jnp.exp(top_b - highest)
    return (
        highest,
        total_a * factor_a + total_b * factor_b,
        weighted_a * factor_a[..., None] + weighted_b * factor_b[..., None],
    )


def local(
    tokens,
    norm_gain,
    w_query,
    w_key,
    w_value,
    w_forget,
    forget_bias,
    key_cache,
    value_cache,
    gate_cache,
    lengths,
    w_out,
):
    batch_rows = tokens.shape[0]
    head_count = gate_cache.shape[1]
    span = gate_cache.shape[2]
    kv_count = key_cache.shape[2] // HEAD_DIM
    groups = head_count // kv_count
    score_scaling = HEAD_DIM ** (-0.5)
    tokens_f = tokens.astype(jnp.float32)
    squares = jnp.sum(tokens_f * tokens_f, axis=1)
    scaled = (tokens_f * norm_gain.astype(jnp.float32)[None, :]).astype(jnp.bfloat16)
    query_part = jnp.dot(scaled, w_query, preferred_element_type=jnp.float32)
    key_part = jnp.dot(scaled, w_key, preferred_element_type=jnp.float32)
    value_part = jnp.dot(scaled, w_value, preferred_element_type=jnp.float32)
    forget_part = jnp.dot(scaled, w_forget, preferred_element_type=jnp.float32)
    query_sum, key_sum, value_sum, forget_sum, square_sum = packed_total(
        (query_part, key_part, value_part, forget_part, squares), KV
    )
    inverse = lax.rsqrt(square_sum / D + EPSILON)
    query_rows = (
        (query_sum * inverse[:, None])
        .astype(jnp.bfloat16)
        .reshape(batch_rows, kv_count, groups, HEAD_DIM)
    )
    key_rows = key_cache.reshape(batch_rows, span, kv_count, HEAD_DIM)
    scores = jnp.einsum("bkgd,bpkd->bkgp", query_rows, key_rows, preferred_element_type=jnp.float32)
    scores = scores.reshape(batch_rows, head_count, span) * score_scaling + gate_cache
    position = lax.axis_index(KV) * span + lax.broadcasted_iota(jnp.int32, (1, 1, span), 2)
    valid = position < lengths[:, None, None]
    scores = jnp.where(valid, scores, NEGATIVE)
    top_score = jnp.max(scores, axis=2)
    weights = jnp.where(valid, jnp.exp(scores - top_score[..., None]), 0.0)
    total = jnp.sum(weights, axis=2)
    weights_low = weights.astype(jnp.bfloat16).reshape(batch_rows, kv_count, groups, span)
    values = value_cache.reshape(batch_rows, span, kv_count, HEAD_DIM)
    weighted = jnp.einsum(
        "bkgp,bpkd->bkgd", weights_low, values, preferred_element_type=jnp.float32
    )
    weighted = weighted.reshape(batch_rows, head_count, HEAD_DIM)
    top_score, total, weighted = merged_by_axis((top_score, total, weighted), KV, combine_parts)
    fresh_key = (
        (key_sum * inverse[:, None]).astype(jnp.bfloat16).reshape(batch_rows, kv_count, HEAD_DIM)
    )
    new_value = (
        (value_sum * inverse[:, None]).astype(jnp.bfloat16).reshape(batch_rows, kv_count, HEAD_DIM)
    )
    forget_logarithm = jax.nn.log_sigmoid(forget_sum * inverse[:, None] + forget_bias[None, :])
    self_token_score = jnp.einsum(
        "cptj,cpj->cpt", query_rows, fresh_key, preferred_element_type=jnp.float32
    )
    self_token_score = (
        self_token_score.reshape(batch_rows, head_count) * score_scaling - forget_logarithm
    )
    highest_all = jnp.maximum(top_score, self_token_score)
    past_factor = jnp.exp(top_score - highest_all)
    own_weight = jnp.exp(self_token_score - highest_all)
    denominator = total * past_factor + own_weight
    own_values = jnp.repeat(new_value.astype(jnp.float32), groups, axis=1)
    attended = (
        weighted * past_factor[..., None] + own_weight[..., None] * own_values
    ) / denominator[..., None]
    attended = attended.astype(jnp.bfloat16).reshape(batch_rows, head_count * HEAD_DIM)
    partial_value = jnp.dot(attended, w_out, preferred_element_type=jnp.float32)
    partial_value = lax.optimization_barrier(partial_value.astype(jnp.bfloat16)).astype(jnp.float32)
    summed = over_copies(partial_value.astype(jnp.bfloat16), "tp").astype(jnp.float32)
    return summed.astype(jnp.bfloat16)


def solution(mesh):
    split = Mesh(mesh.devices.reshape(16, 4, mesh.shape["tp"]), ("kv_0", "kv_1", "tp"))
    return jax.shard_map(
        local,
        mesh=split,
        in_specs=(
            P(None, KV),
            P(KV),
            P(KV, "tp"),
            P(KV, "tp"),
            P(KV, "tp"),
            P(KV, "tp"),
            P("tp"),
            P(None, KV, "tp"),
            P(None, KV, "tp"),
            P(None, "tp", KV),
            P(),
            P("tp", KV),
        ),
        out_specs=P(None, KV),
        check_vma=False,
    )
```

profile of v0, /device:TPU:1, one launch (start us, length us, event | category | flops | bytes accessed | tf_op | source)
XLA Modules:
  0.0 177.8 jit_solution(1243262262476015052)
XLA Ops:
  6.5 0.8 convert_element_type.46
  7.4 0.8 fusion.60
  8.2 0.9 convolution_bitcast_fusion.2
  9.0 0.9 convolution_bitcast_fusion.1
  9.9 0.8 fusion.75
  10.8 1.0 convolution_bitcast_fusion
  12.3 34.1 %all_to_all.20 = f32[64,1,387]{2,1,0:T(1,128)S(1)} all-to-all(f32[64,1,387]{2,1,0:T(1,128)S(1)} %all_to_all.13), channel_id=1, replica_groups=mesh['kv_0'=16,'kv_1'=4,'tp'=8] {'kv_0','kv_1'}, dimensions={0} | all-to-all | bytes 198144 | tf_op jit(solution)/shard_map/all_to_all | solution.py:45
  46.5 0.7 broadcast_in_dim.26
  47.2 6.3 %all-to-all-start.1 = ((f32[64,1,387]{2,1,0:T(1,128)}), f32[64,1,387]{2,1,0:T(1,128)S(1)}, u32[]{:S(2)}, u32[]{:S(2)}) async-start(f32[64,1,387]{2,1,0:T(1,128)} %broadcast_in_dim.26), calls=%async_computation.1 | async-start | bytes 262144 | tf_op jit(solution)/shard_map/all_to_all | solution.py:31
  53.6 14.9 %all-to-all-done.1 = f32[64,1,387]{2,1,0:T(1,128)S(1)} async-done(((f32[64,1,387]{2,1,0:T(1,128)}), f32[64,1,387]{2,1,0:T(1,128)S(1)}, u32[]{:S(2)}, u32[]{:S(2)}) %all-to-all-start.1) | async-done | bytes 99104 | tf_op jit(solution)/shard_map/all_to_all | solution.py:31
  69.2 0.7 fusion.164
  70.3 2.0 %fusion.4 = f32[32,4,128]{2,1,0:T(4,128)S(1)} fusion(bf16[32,256,128]{2,1,0:T(8,128)(2,1)} %param.20, f32[32,4,256]{2,1,0:T(4,128)S(1)} %get-tuple-element.80, f32[32,4]{1,0:T(8,128)S(1)} %get-tuple-element.79, pred[32,256]{1,0:T(8,128)(4,1)S(1)} %broadcast_compare_fusion), kind=kOutput, calls=%fused_computation.12 | convolution fusion | flops 8486912 | bytes 2302464 | tf_op jit(solution)/shard_map/bkgp,bpkd->bkgd/dot_general | solution.py:154
  73.1 3.0 %slice.389 = f32[6192,4]{1,0:T(8,128)} reshape(f32[64,387]{1,0:T(8,128)S(1)} %reduce.2) | data formatting | bytes 198144 | tf_op jit(solution)/shard_map/slice | solution.py:59
  76.3 50.1 %all-gather.6.cloned.1.call-done = f32[16,130,128]{2,1,0:T(8,128)} async-done(((f32[1,130,128]{2,1,0:T(8,128)}), f32[16,130,128]{2,1,0:T(8,128)}) %all-gather.6.cloned.1.call-update) | async-done | bytes 1064976 | tf_op jit(solution)/shard_map/all_gather | solution.py:72
  127.1 0.9 fusion.83
  128.0 0.7 fusion.158
  128.7 0.7 fusion.156
  129.4 0.7 fusion.154
  130.1 0.7 fusion.152
  130.8 0.7 fusion.150
  132.9 1.9 %fusion.11 = f32[128,128]{1,0:T(8,128)S(1)} fusion(f32[16,130,128]{2,1,0:T(8,128)} %all-gather.6.cloned.1.call-done, f32[128]{0:T(128)S(1)} %get-tuple-element.72, f32[128]{0:T(128)S(1)} %get-tuple-element.69, f32[128]{0:T(128)S(1)} %get-tuple-element.71, f32[128]{0:T(128)S(1)} %get-tuple-element.70, f32[128]{0:T(128)S(1)} %get-tuple-element.68, ...), kind=kLoop, calls=%fused_computation.28 | loop fusion | flops 737280 | bytes 1129472 | tf_op jit(solution)/shard_map/add | solution.py:103
  134.8 9.7 %all-gather.3 = f32[4,130,128]{2,1,0:T(8,128)S(1)} all-gather(f32[1,130,128]{2,1,0:T(8,128)S(1)} %maximum_bitcast_fusion.1), channel_id=3, replica_groups=mesh['kv_0'=16,'kv_1'=4,'tp'=8] {'kv_1'}, dimensions={0}, use_global_device_ids=true | all-gather | bytes 332800 | tf_op jit(solution)/shard_map/all_gather | solution.py:72
  145.6 0.8 multiply_add_fusion
  147.6 22.6 %all_to_all.21 = bf16[8,2,1024]{2,1,0:T(2,128)(2,1)S(1)} all-to-all(bf16[8,2,1024]{2,1,0:T(2,128)(2,1)S(1)} %reshape.2216), channel_id=1, replica_groups=mesh['kv_0'=16,'kv_1'=4,'tp'=8] {'tp'}, dimensions={0} | all-to-all | bytes 65536 | tf_op jit(solution)/shard_map/all_to_all | solution.py:31
  (63 shorter events, 7.5 us)
Async XLA Ops:
  6.5 62.6 %copy-start = (bf16[32,256,128]{2,1,0:T(8,128)(2,1)S(1)}, bf16[32,256,128]{2,1,0:T(8,128)(2,1)}, u32[]{:S(2)}) copy-start(bf16[32,256,128]{2,1,0:T(8,128)(2,1)} %param.19) | copy-start | bytes 6291460
  6.5 47.0 %copy-start.4 = (s32[32]{0:T(128)S(1)}, s32[32]{0:T(128)}, u32[]{:S(2)}) copy-start(s32[32]{0:T(128)} %param.22) | copy-start | bytes 388
  10.8 58.4 %copy-start.1 = (f32[32,4,256]{2,1,0:T(4,128)S(1)}, f32[32,4,256]{2,1,0:T(4,128)}, u32[]{:S(2)}) copy-start(f32[32,4,256]{2,1,0:T(4,128)} %param.21) | copy-start | bytes 393220
  47.2 21.3 %all-to-all-start.1 = ((f32[64,1,387]{2,1,0:T(1,128)}), f32[64,1,387]{2,1,0:T(1,128)S(1)}, u32[]{:S(2)}, u32[]{:S(2)}) async-start(f32[64,1,387]{2,1,0:T(1,128)} %broadcast_in_dim.26), calls=%async_computation.1 | async-start | bytes 262144 | tf_op jit(solution)/shard_map/all_to_all | solution.py:31
  53.5 73.0 %all-gather.6.cloned.1.call-start = ((), (), s32[]{:S(2)}) async-start(), calls=%async_computation.3 | async-start | bytes 1183744 | tf_op jit(solution)/shard_map/all_gather | solution.py:72
  134.8 10.8 %copy-start.3 = (f32[4]{0:T(128)S(1)}, f32[4]{0:T(128)}, u32[]{:S(2)}) copy-start(f32[4]{0:T(128)} %param.18) | copy-start | bytes 52
  144.6 2.7 %copy-start.2 = (bf16[512,64]{0,1:T(8,128)(2,1)S(1)}, bf16[512,64]{0,1:T(8,128)(2,1)}, u32[]{:S(2)}) copy-start(bf16[512,64]{0,1:T(8,128)(2,1)} %param.23) | copy-start | bytes 196612
Sparse Core Ops, SparseCore 0:
  73.2 53.1 all-gather.5
where the time goes:
time: 179 us; the launch traced here: 178 us
  blocking collectives  66.5 us (37%)
  waiting for transfers between devices  65.1 us (36%)
  between operations  13.8 us (8%)
  other arithmetic  13.1 us (7%)
  matrix products  6.63 us (4%)
  local copies, waits for them, and re-layouts  6.51 us (4%)
  starting transfers between devices  6.29 us (4%)
    all_gather x1, waiting for transfers between devices, gathered_once(): both, at, found = (lax.all_gather(jnp.concatenate(lines), axis), 0, {})  50.1 us
    all_to_all x1, blocking collectives, summed_on_arrival(): lax.all_to_all(tiles, axis, split_axis=0, concat_axis=0, tiled=True)  34.1 us
    all_to_all x1, blocking collectives, copy_for_each(): lax.all_to_all(jnp.broadcast_to(x[None], (size, *x.shape)), axis, 0, 0, t...  22.6 us
    all_to_all x1, waiting for transfers between devices, copy_for_each(): lax.all_to_all(jnp.broadcast_to(x[None], (size, *x.shape)), axis, 0, 0, t...  14.9 us
    all_gather x1, blocking collectives, gathered_once(): both, at, found = (lax.all_gather(jnp.concatenate(lines), axis), 0, {})  9.75 us
    all_to_all x1, starting transfers between devices, copy_for_each(): lax.all_to_all(jnp.broadcast_to(x[None], (size, *x.shape)), axis, 0, 0, t...  6.25 us
    exp x7, other arithmetic, combine_parts(): factor_b = jnp.exp(top_b - highest)  4.9 us
  transfers between devices with their start and end apart: 2, of which 2 were waited for; matrix products, arithmetic and copies ran while one was open for 2% of the time, Pallas kernels for 0%

commit v1 on v0

v1 whole, which is shorter than its diff:
```python
import functools

import jax
import jax.numpy as jnp
from jax import lax
from jax.experimental import pallas as pl
from jax.experimental.pallas import tpu as pltpu
from jax.sharding import PartitionSpec as P

HEAD_DIM = 128
ROWS = 8
HEADS = 4
NY = 4
EPSILON = 1e-06
NEGATIVE = -1e30
MESH = pl.DeviceIdType.MESH
NEAR = (-1, 0, 1, 2)


def kernel(
    nz, ny, ntp,
    tokens, gain, w_query, w_key, w_value, w_forget, bias, keys, values, gates, lengths, w_out,
    out,
    tok_v, gain_v, wq_v, wk_v, wv_v, wf_v, wo_v, k_v, v_v, g_v,
    part, ry, acc, sqrow, qz, sqz, kvz, q_all, gp,
    bsend, by, bacc, bstat, bz, bsz, at, ot,
    in_sem, kv_sem, send, recv,
):
    kv, tp = lax.axis_index("kv"), lax.axis_index("tp")
    z, y = kv // ny, lax.rem(kv, ny)
    mine = lax.rem(z, HEADS)
    depth = nz * ny * tokens.shape[1]
    span = keys.shape[1]
    scaling = HEAD_DIM ** (-0.5)

    def at_y(d):
        return (z * ny + lax.rem(y + d, ny), tp)

    def at_z(d):
        return (lax.rem(z + d, nz) * ny + y, tp)

    def at_tp(d):
        return (kv, lax.rem(tp + d, ntp))

    barrier = pltpu.get_barrier_semaphore()
    far_first = sorted(range(1, nz), key=lambda d: -min(d, nz - d))
    for d in far_first:
        pl.semaphore_signal(barrier, inc=1, device_id=at_z(d), device_id_type=MESH)
    for d in range(1, ny):
        pl.semaphore_signal(barrier, inc=1, device_id=at_y(d), device_id_type=MESH)
    for d in range(1, ntp):
        pl.semaphore_signal(barrier, inc=1, device_id=at_tp(d), device_id_type=MESH)

    loads = [
        pltpu.make_async_copy(a, b, in_sem.at[i])
        for i, (a, b) in enumerate(
            (
                (tokens, tok_v), (gain, gain_v), (w_query, wq_v), (w_key, wk_v), (w_value, wv_v),
                (w_forget, wf_v), (gates, g_v),
                (w_out, wo_v.at[0:64]), (w_out, wo_v.at[64:128]),
            )
        )
    ]
    for c in loads:
        c.start()
    k_load = pltpu.make_async_copy(keys, k_v, kv_sem.at[0])
    v_load = pltpu.make_async_copy(values, v_v, kv_sem.at[1])
    k_load.start()
    v_load.start()

    def remote(src, dst, phase, peer):
        return pltpu.make_async_remote_copy(
            src_ref=src, dst_ref=dst, send_sem=send.at[phase], recv_sem=recv.at[phase],
            device_id=peer, device_id_type=MESH,
        )

    def arrived(ref, phase):
        pltpu.make_async_copy(ref, ref, recv.at[phase]).wait()

    def left(ref, phase):
        pltpu.make_async_copy(ref, ref, send.at[phase]).wait()

    lane = lax.broadcasted_iota(jnp.int32, (ROWS, HEAD_DIM), 1)
    row = lax.broadcasted_iota(jnp.int32, (ROWS, HEAD_DIM), 0)
    eye = lane == row

    def as_row(column):
        return jnp.sum(jnp.where(eye, jnp.broadcast_to(column, (ROWS, HEAD_DIM)), 0.0), axis=0, keepdims=True)

    def as_column(line):
        return jnp.sum(jnp.where(eye, jnp.broadcast_to(line, (ROWS, HEAD_DIM)), 0.0), axis=1, keepdims=True)

    for c in loads[:6]:
        c.wait()
    x = tok_v[...].astype(jnp.float32)
    squares = jnp.sum(x * x, axis=1, keepdims=True)
    scaled = (x * gain_v[...].astype(jnp.float32)).astype(jnp.bfloat16)
    for t in range(HEADS):
        p = jnp.dot(scaled, wq_v[:, t * HEAD_DIM : (t + 1) * HEAD_DIM], preferred_element_type=jnp.float32)
        for j in range(ny):
            part[j, t] = p[j * ROWS : (j + 1) * ROWS]
    for t, w in ((4, wk_v), (5, wv_v)):
        p = jnp.dot(scaled, w[...], preferred_element_type=jnp.float32)
        for j in range(ny):
            part[j, t] = p[j * ROWS : (j + 1) * ROWS]
    p = lax.dot_general(scaled, wf_v[...], (((1,), (1,)), ((), ())), preferred_element_type=jnp.float32)
    for j in range(ny):
        side = jnp.broadcast_to(squares[j * ROWS : (j + 1) * ROWS], (ROWS, HEAD_DIM))
        for n in range(HEADS):
            f = jnp.broadcast_to(p[j * ROWS : (j + 1) * ROWS, n : n + 1], (ROWS, HEAD_DIM))
            side = jnp.where(lane == n, f, side)
        part[j, 6] = side

    pl.semaphore_wait(barrier, nz - 1 + ny - 1 + ntp - 1)

    for d in range(1, ny):
        remote(part.at[lax.rem(y + d, ny)], ry.at[d - 1], 0, at_y(d)).start()

    loads[6].wait()
    position = kv * span + lax.broadcasted_iota(jnp.int32, (1, span), 1)
    for j in range(ny):
        for i in range(ROWS):
            b = j * ROWS + i
            valid = position < lengths[b]
            for n in range(HEADS):
                gp[j, n * ROWS + i : n * ROWS + i + 1, :] = jnp.where(valid, g_v[b, n : n + 1, :], NEGATIVE)

    arrived(ry, 0)
    for t in range(7):
        total = part[y, t]
        for d in range(ny - 1):
            total = total + ry[d, t]
        acc[t] = total
    sqrow[...] = as_row(acc[6][:, HEADS : HEADS + 1])

    for d in far_first:
        target = lax.rem(z + d, nz)
        remote(acc.at[lax.rem(target, HEADS)], qz.at[d - 1], 1, at_z(d)).start()
        remote(sqrow, sqz.at[d - 1], 2, at_z(d)).start()

    for d in range(1, nz):
        @pl.when(z == d)
        def _(d=d):
            remote(acc.at[4:7], kvz.at[d - 1], 3, (y, tp)).start()

    arrived(sqz, 2)
    line = sqrow[...]
    for d in range(nz - 1):
        line = line + sqz[d]
    inverse = lax.rsqrt(as_column(line) / depth + EPSILON)
    arrived(qz, 1)
    total = acc[mine]
    for d in range(nz - 1):
        total = total + qz[d]
    slot = y * HEADS + mine
    q_all[slot] = (total * inverse).astype(jnp.bfloat16)

    def spread(ref, slot, phase):
        peers = [(-o, d) for o in NEAR for d in range(ny) if (o, d) != (0, 0)]
        for dz, dy in sorted(peers, key=lambda t: -abs(t[0]) - min(t[1], ny - t[1])):
            peer = (lax.rem(z + dz + nz, nz) * ny + lax.rem(y + dy, ny), tp)
            remote(ref.at[slot], ref.at[slot], phase, peer).start()

    spread(q_all, slot, 4)
    k_load.wait()
    v_load.wait()
    arrived(q_all.at[pl.ds(0, HEADS * ny - 1)], 4)

    tall = lax.rem(lax.broadcasted_iota(jnp.int32, (HEADS * ROWS, 1), 0), ROWS)
    for d in tuple(range(ny // 2, ny)) + tuple(range(1, ny // 2)) + (0,):
        j = lax.rem(y + d, ny)
        q = jnp.concatenate([q_all[j * HEADS + n] for n in range(HEADS)], axis=0)
        scores = jnp.zeros((HEADS * ROWS, span), jnp.float32)
        for i in range(ROWS):
            s = lax.dot_general(q, k_v[j * ROWS + i], (((1,), (1,)), ((), ())), preferred_element_type=jnp.float32)
            scores = jnp.where(tall == i, s, scores)
        scores = scores * scaling + gp[j]
        top = jnp.max(scores, axis=1, keepdims=True)
        weights = jnp.exp(scores - top)
        summed = jnp.sum(weights, axis=1, keepdims=True)
        found = jnp.zeros((HEADS * ROWS, HEAD_DIM), jnp.float32)
        for i in range(ROWS):
            w = jnp.where(tall == i, weights, 0.0).astype(jnp.bfloat16)
            found = found + jnp.dot(w, v_v[j * ROWS + i], preferred_element_type=jnp.float32)
        wide = lax.broadcasted_iota(jnp.int32, (HEADS * ROWS, HEAD_DIM), 1)
        bsend[d, 0] = found
        bsend[d, 1] = jnp.where(wide == 0, top, summed)
        if d:
            remote(bsend.at[d], by.at[d - 1], 5, at_y(d)).start()

    arrived(by, 5)
    tops = [bsend[0, 1][:, 0:1]] + [by[d, 1][:, 0:1] for d in range(ny - 1)]
    top = functools.reduce(jnp.maximum, tops)
    summed = jnp.zeros_like(top)
    found = jnp.zeros((HEADS * ROWS, HEAD_DIM), jnp.float32)
    for k in range(ny):
        block = bsend.at[0] if k == 0 else by.at[k - 1]
        factor = jnp.exp(tops[k] - top)
        summed = summed + block[1][:, 1:2] * factor
        found = found + block[0] * factor
    for n in range(HEADS):
        bacc[n] = found[n * ROWS : (n + 1) * ROWS]
        bstat[n, 0:1] = as_row(top[n * ROWS : (n + 1) * ROWS])
        bstat[n, 1:2] = as_row(summed[n * ROWS : (n + 1) * ROWS])

    @pl.when(z == 0)
    def _():
        arrived(kvz, 3)
        new = [acc[4 + t] for t in range(3)]
        for d in range(nz - 1):
            new = [new[t] + kvz[d, t] for t in range(3)]
        rate = lax.rsqrt(as_column(line) / depth + EPSILON)
        new_key = (new[0] * rate).astype(jnp.bfloat16).astype(jnp.float32)
        new_value = (new[1] * rate).astype(jnp.bfloat16).astype(jnp.float32)
        for n in range(HEADS):
            forget = new[2][:, n : n + 1] * rate + bias[n]
            log_forget = jnp.minimum(forget, 0.0) - jnp.log1p(jnp.exp(-jnp.abs(forget)))
            query = q_all[y * HEADS + n].astype(jnp.float32)
            own = jnp.sum(query * new_key, axis=1, keepdims=True) * scaling - log_forget
            old = top[n * ROWS : (n + 1) * ROWS]
            higher = jnp.maximum(old, own)
            past, now = jnp.exp(old - higher), jnp.exp(own - higher)
            bacc[n] = found[n * ROWS : (n + 1) * ROWS] * past + new_value * now
            bstat[n, 0:1] = as_row(higher)
            bstat[n, 1:2] = as_row(summed[n * ROWS : (n + 1) * ROWS] * past + now)

    for d in far_first:
        target = lax.rem(lax.rem(z + d, nz), HEADS)
        remote(bacc.at[target], bz.at[d - 1], 6, at_z(d)).start()
        remote(bstat.at[target], bsz.at[d - 1], 7, at_z(d)).start()
    arrived(bsz, 7)
    stats = [bstat[mine]] + [bsz[d] for d in range(nz - 1)]
    top = functools.reduce(jnp.maximum, [s[0:1] for s in stats])
    factors = [jnp.exp(s[0:1] - top) for s in stats]
    summed = functools.reduce(jnp.add, [s[1:2] * f for s, f in zip(stats, factors)])
    shares = [as_column(f / summed) for f in factors]
    arrived(bz, 6)
    found = bacc[mine] * shares[0]
    for d in range(nz - 1):
        found = found + bz[d] * shares[d + 1]
    slot = mine * ny + y
    at[slot] = found.astype(jnp.bfloat16)
    spread(at, slot, 8)
    loads[7].wait()
    loads[8].wait()
    arrived(at.at[pl.ds(0, HEADS * ny - 1)], 8)

    total = jnp.zeros((ny * ROWS, 2 * 64), jnp.float32)
    for n in range(HEADS):
        a = jnp.concatenate([at[n * ny + j] for j in range(ny)], axis=0)
        total = total + lax.dot_general(
            a, wo_v[:, n * HEAD_DIM : (n + 1) * HEAD_DIM], (((1,), (1,)), ((), ())), preferred_element_type=jnp.float32
        )
    half = ny * ROWS // 2
    low = lax.broadcasted_iota(jnp.int32, (half, 2 * 64), 1) < 64
    ot[0] = jnp.where(low, total[:half], total[half:]).astype(jnp.bfloat16)
    for d in range(1, ntp):
        remote(ot.at[0], ot.at[d], 9, at_tp(d)).start()
    arrived(ot.at[pl.ds(1, ntp - 1)], 9)
    total = ot[0].astype(jnp.float32)
    for d in range(1, ntp):
        total = total + ot[d].astype(jnp.float32)
    out[0:half] = total[:, 0:64].astype(jnp.bfloat16)
    out[half:] = total[:, 64:].astype(jnp.bfloat16)

    left(ry, 0)
    left(qz, 1)
    left(sqz, 2)
    @pl.when(z != 0)
    def _():
        left(acc.at[4:7], 3)
    left(q_all.at[pl.ds(0, HEADS * ny - 1)], 4)
    left(by, 5)
    left(bz, 6)
    left(bsz, 7)
    left(at.at[pl.ds(0, HEADS * ny - 1)], 8)
    left(ot.at[pl.ds(1, ntp - 1)], 9)


def local(
    nz, ny, ntp,
    tokens, norm_gain, w_query, w_key, w_value, w_forget, forget_bias, key_cache, value_cache, gate_cache, lengths, w_out,
):
    f32, bf16 = jnp.float32, jnp.bfloat16
    rows, span = key_cache.shape[0], key_cache.shape[1]
    wide = HEAD_DIM * HEADS
    args = (
        tokens, norm_gain.reshape(1, -1), w_query, w_key, w_value, w_forget.T, forget_bias,
        key_cache, value_cache, gate_cache, lengths, w_out.T,
    )
    specs = [pl.BlockSpec(memory_space=pl.ANY)] * 12
    specs[6] = specs[10] = pl.BlockSpec(memory_space=pltpu.SMEM)
    own = tokens.shape[1]
    scratch = [
        pltpu.VMEM((rows, own), bf16), pltpu.VMEM((1, own), bf16), pltpu.VMEM((own, wide), bf16),
        pltpu.VMEM((own, HEAD_DIM), bf16), pltpu.VMEM((own, HEAD_DIM), bf16), pltpu.VMEM((HEADS, own), bf16),
        pltpu.VMEM((2 * 64, wide), bf16), pltpu.VMEM((rows, span, HEAD_DIM), bf16), pltpu.VMEM((rows, span, HEAD_DIM), bf16),
        pltpu.VMEM((rows, HEADS, span), f32),
        pltpu.VMEM((ny, 7, ROWS, HEAD_DIM), f32),
        pltpu.VMEM((ny - 1, 7, ROWS, HEAD_DIM), f32),
        pltpu.VMEM((7, ROWS, HEAD_DIM), f32),
        pltpu.VMEM((1, HEAD_DIM), f32),
        pltpu.VMEM((nz - 1, ROWS, HEAD_DIM), f32),
        pltpu.VMEM((nz - 1, 1, HEAD_DIM), f32),
        pltpu.VMEM((nz - 1, 3, ROWS, HEAD_DIM), f32),
        pltpu.VMEM((ny * HEADS, ROWS, HEAD_DIM), bf16),
        pltpu.VMEM((ny, HEADS * ROWS, span), f32),
        pltpu.VMEM((ny, 2, HEADS * ROWS, HEAD_DIM), f32),
        pltpu.VMEM((ny - 1, 2, HEADS * ROWS, HEAD_DIM), f32),
        pltpu.VMEM((HEADS, ROWS, HEAD_DIM), f32),
        pltpu.VMEM((HEADS, 2, HEAD_DIM), f32),
        pltpu.VMEM((nz - 1, ROWS, HEAD_DIM), f32),
        pltpu.VMEM((nz - 1, 2, HEAD_DIM), f32),
        pltpu.VMEM((HEADS * ny, ROWS, HEAD_DIM), bf16),
        pltpu.VMEM((ntp, ny * ROWS // 2, 2 * 64), bf16),
        pltpu.SemaphoreType.DMA((9,)), pltpu.SemaphoreType.DMA((2,)),
        pltpu.SemaphoreType.DMA((10,)), pltpu.SemaphoreType.DMA((10,)),
    ]
    return pl.pallas_call(
        functools.partial(kernel, nz, ny, ntp),
        out_shape=jax.ShapeDtypeStruct((rows, w_out.shape[1]), bf16),
        in_specs=specs,
        out_specs=pl.BlockSpec(memory_space=pltpu.VMEM),
        scratch_shapes=scratch,
        compiler_params=pltpu.CompilerParams(collective_id=0, has_side_effects=True),
        name="step",
    )(*args)


def solution(mesh):
    ny, ntp = NY, mesh.shape["tp"]
    nz = mesh.shape["kv"] // ny
    return jax.shard_map(
        functools.partial(local, nz, ny, ntp),
        mesh=mesh,
        in_specs=(
            P(None, "kv"), P("kv"), P("kv", "tp"), P("kv", "tp"), P("kv", "tp"), P("kv", "tp"), P("tp"),
            P(None, "kv", "tp"), P(None, "kv", "tp"), P(None, "tp", "kv"), P(), P("tp", "kv"),
        ),
        out_specs=P(None, "kv"),
        check_vma=False,
    )
```

time: 179 us -> 57.5 us (0.32)
  blocking collectives: 66.5 us -> 0 us
  waiting for transfers between devices: 65.1 us -> 0 us
  Pallas kernels: 0 us -> 55.9 us
  between operations: 13.8 us -> 0.01 us
  other arithmetic: 13.1 us -> 0 us
  matrix products: 6.63 us -> 0 us
  starting transfers between devices: 6.29 us -> 0 us
  local copies, waits for them, and re-layouts: 6.51 us -> 1.3 us
    all_to_all x2 -> x0, blocking collectives: 56.7 us -> none  [the longest x1 34.1 us: summed_on_arrival(): lax.all_to_all(tiles, axis, split_axis=0, concat_axis=0, tiled=True)]
    pallas_call x0 -> x1, Pallas kernels: none -> 55.9 us  [local(): pl.pallas_call(functools.partial(kernel, nz, ny, ntp), out_shape=jax.Shap...]
    all_gather x1 -> x0, waiting for transfers between devices: 50.1 us -> none  [gathered_once(): both, at, found = (lax.all_gather(jnp.concatenate(lines), axis), 0, {})]
    all_to_all x1 -> x0, waiting for transfers between devices: 14.9 us -> none  [copy_for_each(): lax.all_to_all(jnp.broadcast_to(x[None], (size, *x.shape)), axis, 0, 0, t...]
    all_gather x1 -> x0, blocking collectives: 9.75 us -> none  [gathered_once(): both, at, found = (lax.all_gather(jnp.concatenate(lines), axis), 0, {})]
    dot_general x8 -> x0, matrix products: 6.63 us -> none  [the longest x1 2.03 us: local(): jnp.einsum('bkgp,bpkd->bkgd', weights_low, values, preferred_element_type...]
    all_to_all x1 -> x0, starting transfers between devices: 6.25 us -> none  [copy_for_each(): lax.all_to_all(jnp.broadcast_to(x[None], (size, *x.shape)), axis, 0, 0, t...]
    exp x8 -> x0, other arithmetic: 5.59 us -> none  [the longest x7 4.9 us: combine_parts(): factor_b = jnp.exp(top_b - highest)]
  transfers between devices with their start and end apart: 2 -> 0, of which waited for: 2 -> 0; matrix products, arithmetic and copies ran while one was open for 2% -> 0% of each run, Pallas kernels for 0% -> 0%
where the time goes in v1:
time: 57.5 us; the launch traced here: 57.2 us
  Pallas kernels  55.9 us (97%)
  local copies, waits for them, and re-layouts  1.3 us (2%)
    pallas_call x1, Pallas kernels, local(): pl.pallas_call(functools.partial(kernel, nz, ny, ntp), out_shape=jax.Shap...  55.9 us
    unnamed x1, local copies, waits for them, and re-layouts  1.3 us

profile of v1, /device:TPU:1, one launch (start us, length us, event | category | flops | bytes accessed | tf_op | source)
XLA Modules:
  0.0 57.2 jit_solution(16349229356565675085)
XLA Ops:
  0.0 55.9 %step.1 = bf16[32,64]{1,0:T(8,128)(2,1)} custom-call(bf16[32,64]{1,0:T(8,128)(2,1)} %tokens.1, bf16[1,64]{1,0:T(2,128)(2,1)} %bitcast.5, bf16[64,512]{1,0:T(8,128)(2,1)} %w_query.1, bf16[64,128]{1,0:T(8,128)(2,1)} %w_key.1, bf16[64,128]{1,0:T(8,128)(2,1)} %w_value.1, bf16[4,64]{1,0:T(4,128)(2,1)} %bitcast.4, f32[4]{0:T(128)} %bias.1, ...), custom_call_target="tpu_custom_call" | custom-call | tf_op jit(solution)/shard_map/step/pallas_call | solution.py:319
  55.9 1.3 %copy.14 = bf16[32,64]{1,0:T(8,128)(2,1)} copy(bf16[32,64]{1,0:T(8,128)(2,1)} %step.1) | data formatting | bytes 8192

commit v2 on v1

v2 whole, which is shorter than its diff:
```python
import functools

import jax
import jax.numpy as jnp
from jax import lax
from jax.experimental import pallas as pl
from jax.experimental.pallas import tpu as pltpu
from jax.sharding import PartitionSpec as P

HEAD_DIM = 128
ROWS = 8
HEADS = 4
NY = 4
EPSILON = 1e-06
NEGATIVE = -1e30
MESH = pl.DeviceIdType.MESH
NEAR = (-1, 0, 1, 2)


def kernel(
    nz, ny, ntp,
    tokens, gain, w_query, w_key, w_value, w_forget, bias, keys, values, gates, lengths, w_out,
    out,
    tok_v, gain_v, wq_v, wk_v, wv_v, wf_v, wo_v, k_v, v_v, g_v, bias_s, len_s,
    part, ry, acc, sqrow, qz, sqz, kvz, q_all, gp,
    bsend, bstat, by, bys, bz, bsz, own_s, value_s, ots, ot,
    in_sem, send, recv, here,
):
    kv, tp = lax.axis_index("kv"), lax.axis_index("tp")
    z, y = kv // ny, lax.rem(kv, ny)
    mine = lax.rem(z, HEADS)
    depth = nz * ny * tokens.shape[1]
    span = keys.shape[1]
    columns = w_out.shape[0]
    scaling = HEAD_DIM ** (-0.5)

    def turned(i, d, n):
        return jnp.where(i + d < n, i + d, i + d - n)

    def at_y(d):
        return (z * ny + turned(y, d, ny), tp)

    def at_z(d):
        return (turned(z, d, nz) * ny + y, tp)

    loads = [
        pltpu.make_async_copy(a, b, in_sem.at[i])
        for i, (a, b) in enumerate(
            (
                (tokens, tok_v), (gain, gain_v), (w_query, wq_v), (w_key, wk_v), (w_value, wv_v),
                (w_forget, wf_v), (lengths, len_s), (gates, g_v), (bias, bias_s), (keys, k_v), (values, v_v),
                (w_out, wo_v.at[pl.ds(pl.multiple_of(y * columns, columns), columns)]),
            )
        )
    ]
    for c in loads:
        c.start()

    half = nz // 2

    def rank_of(i):
        return i if i < half else nz - 1 + half - i

    rank = jnp.where(z < half, z, nz - 1 + half - z)
    barrier = pltpu.get_barrier_semaphore()
    meetings = (
        [(rank, rank_of(i), (i * ny + y, tp), 0) for i in sorted(range(nz), key=rank_of, reverse=True)]
        + [(y, i, (z * ny + i, tp), 1) for i in range(ny)]
        + [(tp, i, (kv, i), 2) for i in range(ntp)]
    )
    for me, other, peer, _ in meetings:
        @pl.when(me < other)
        def _(peer=peer):
            pl.semaphore_signal(barrier, inc=1, device_id=peer, device_id_type=MESH)
    earlier = rank + y + tp

    @pl.when(earlier > 0)
    def _():
        pl.semaphore_wait(barrier, earlier)

    for kind in range(3):
        pl.semaphore_signal(here.at[kind], inc=1)
    for me, other, peer, kind in meetings:
        @pl.when(me > other)
        def _(peer=peer, kind=kind):
            pl.semaphore_signal(here.at[kind], inc=1, device_id=peer, device_id_type=MESH)

    def remote(src, dst, phase, peer):
        return pltpu.make_async_remote_copy(
            src_ref=src, dst_ref=dst, send_sem=send.at[phase], recv_sem=recv.at[phase],
            device_id=peer, device_id_type=MESH,
        )

    def arrived(ref, phase):
        pltpu.make_async_copy(ref, ref, recv.at[phase]).wait()

    def left(ref, phase):
        pltpu.make_async_copy(ref, ref, send.at[phase]).wait()

    def diagonal(rows):
        shape = (rows, HEAD_DIM)
        return lax.broadcasted_iota(jnp.int32, shape, 1) == lax.broadcasted_iota(jnp.int32, shape, 0)

    def as_row(column):
        return jnp.sum(jnp.where(diagonal(column.shape[0]), column, 0.0), axis=0, keepdims=True)

    def as_column(line, rows):
        return jnp.sum(jnp.where(diagonal(rows), line, 0.0), axis=1, keepdims=True)

    lane = lax.broadcasted_iota(jnp.int32, (ROWS, HEAD_DIM), 1)
    tall_rows = HEADS * ROWS

    for c in loads[:6]:
        c.wait()
    x = tok_v[...].astype(jnp.float32)
    squares = jnp.sum(x * x, axis=1, keepdims=True)
    scaled = (x * gain_v[...].astype(jnp.float32)).astype(jnp.bfloat16)
    for t in range(HEADS):
        p = jnp.dot(scaled, wq_v[:, t * HEAD_DIM : (t + 1) * HEAD_DIM], preferred_element_type=jnp.float32)
        for j in range(ny):
            part[j, t] = p[j * ROWS : (j + 1) * ROWS]
    for t, w in ((4, wk_v), (5, wv_v)):
        p = jnp.dot(scaled, w[...], preferred_element_type=jnp.float32)
        for j in range(ny):
            part[j, t] = p[j * ROWS : (j + 1) * ROWS]
    p = lax.dot_general(scaled, wf_v[...], (((1,), (1,)), ((), ())), preferred_element_type=jnp.float32)
    for j in range(ny):
        side = jnp.broadcast_to(squares[j * ROWS : (j + 1) * ROWS], (ROWS, HEAD_DIM))
        for n in range(HEADS):
            f = jnp.broadcast_to(p[j * ROWS : (j + 1) * ROWS, n : n + 1], (ROWS, HEAD_DIM))
            side = jnp.where(lane == n, f, side)
        part[j, 6] = side

    pl.semaphore_wait(here.at[1], ny - y)
    for d in range(1, ny):
        remote(part.at[turned(y, d, ny)], ry.at[d - 1], 0, at_y(d)).start()

    loads[6].wait()
    loads[7].wait()
    position = kv * span + lax.broadcasted_iota(jnp.int32, (1, span), 1)
    for j in range(ny):
        for i in range(ROWS):
            b = j * ROWS + i
            valid = position < len_s[b]
            for n in range(HEADS):
                gp[j, n * ROWS + i : n * ROWS + i + 1, :] = jnp.where(valid, g_v[b, n : n + 1, :], NEGATIVE)

    arrived(ry, 0)
    for t in range(7):
        total = part[y, t]
        for d in range(ny - 1):
            total = total + ry[d, t]
        acc[t] = total
    sqrow[...] = as_row(acc[6][:, HEADS : HEADS + 1])

    pl.semaphore_wait(here.at[0], nz - rank)
    far_first = sorted(range(1, nz), key=lambda d: -min(d, nz - d))
    for d in far_first:
        remote(acc.at[lax.rem(turned(z, d, nz), HEADS)], qz.at[d - 1], 1, at_z(d)).start()
        remote(sqrow, sqz.at[d - 1], 2, at_z(d)).start()

    for d in range(1, nz):
        @pl.when(z == d)
        def _(d=d):
            remote(acc.at[4:7], kvz.at[d - 1], 3, (y, tp)).start()

    loads[11].wait()
    own_columns = wo_v.at[pl.ds(pl.multiple_of(y * columns, columns), columns)]
    for d in range(1, ny):
        remote(own_columns, own_columns, 4, at_y(d)).start()
    pl.semaphore_wait(here.at[2], ntp - tp)
    for d in range(1, ntp):
        pl.semaphore_signal(here.at[3], inc=1, device_id=(kv, turned(tp, d, ntp)), device_id_type=MESH)

    arrived(sqz, 2)
    line = sqrow[...]
    for d in range(nz - 1):
        line = line + sqz[d]
    rate = lax.rsqrt(as_column(line, ROWS) / depth + EPSILON)
    arrived(qz, 1)
    total = acc[mine]
    for d in range(nz - 1):
        total = total + qz[d]
    slot = y * HEADS + mine
    q_all[slot] = (total * rate).astype(jnp.bfloat16)
    near = [(-o, d) for o in NEAR for d in range(ny) if (o, d) != (0, 0)]
    for dz, dy in sorted(near, key=lambda t: -abs(t[0]) - min(t[1], ny - t[1])):
        peer = (turned(z, dz % nz, nz) * ny + turned(y, dy, ny), tp)
        remote(q_all.at[slot], q_all.at[slot], 5, peer).start()
    loads[9].wait()
    loads[10].wait()
    arrived(q_all.at[pl.ds(0, HEADS * ny - 1)], 5)

    tall = lax.rem(lax.broadcasted_iota(jnp.int32, (tall_rows, 1), 0), ROWS)
    for d in tuple(range(ny // 2, ny)) + tuple(range(1, ny // 2)) + (0,):
        j = turned(y, d, ny)
        q = jnp.concatenate([q_all[j * HEADS + n] for n in range(HEADS)], axis=0)
        scores = jnp.zeros((tall_rows, span), jnp.float32)
        for i in range(ROWS):
            s = lax.dot_general(q, k_v[j * ROWS + i], (((1,), (1,)), ((), ())), preferred_element_type=jnp.float32)
            scores = jnp.where(tall == i, s, scores)
        scores = scores * scaling + gp[j]
        top = jnp.max(scores, axis=1, keepdims=True)
        weights = jnp.exp(scores - top)
        summed = jnp.sum(weights, axis=1, keepdims=True)
        found = jnp.zeros((tall_rows, HEAD_DIM), jnp.float32)
        for i in range(ROWS):
            w = jnp.where(tall == i, weights, 0.0).astype(jnp.bfloat16)
            found = found + jnp.dot(w, v_v[j * ROWS + i], preferred_element_type=jnp.float32)
        top, summed = as_row(top), as_row(summed)
        if d:
            bsend[d - 1] = found.astype(jnp.bfloat16)
            bstat[d - 1, 0:1] = top
            bstat[d - 1, 1:2] = summed
            remote(bsend.at[d - 1], by.at[d - 1], 6, at_y(d)).start()
            remote(bstat.at[d - 1], bys.at[d - 1], 7, at_y(d)).start()

    @pl.when(z == 0)
    def _():
        loads[8].wait()
        arrived(kvz, 3)
        new = [acc[4 + t] for t in range(3)]
        for d in range(nz - 1):
            new = [new[t] + kvz[d, t] for t in range(3)]
        new_key = (new[0] * rate).astype(jnp.bfloat16).astype(jnp.float32)
        value_s[...] = (new[1] * rate).astype(jnp.bfloat16).astype(jnp.float32)
        own = []
        for n in range(HEADS):
            forget = new[2][:, n : n + 1] * rate + bias_s[n]
            log_forget = jnp.minimum(forget, 0.0) - jnp.log1p(jnp.exp(-jnp.abs(forget)))
            query = q_all[y * HEADS + n].astype(jnp.float32)
            own.append(jnp.sum(query * new_key, axis=1, keepdims=True) * scaling - log_forget)
        own_s[...] = as_row(jnp.concatenate(own, axis=0))

    @pl.when(z != 0)
    def _():
        loads[8].wait()

    arrived(bys, 7)
    tops = [top] + [bys[d, 0:1] for d in range(ny - 1)]
    sums = [summed] + [bys[d, 1:2] for d in range(ny - 1)]
    top = functools.reduce(jnp.maximum, tops)
    factors = [jnp.exp(t - top) for t in tops]
    summed = functools.reduce(jnp.add, [s * f for s, f in zip(sums, factors)])
    shares = [as_column(f, tall_rows) for f in factors]
    arrived(by, 6)
    found = found * shares[0]
    for d in range(ny - 1):
        found = found + by[d].astype(jnp.float32) * shares[d + 1]
    last = ny - 1
    bsend[last] = found.astype(jnp.bfloat16)
    bstat[last, 0:1] = top
    bstat[last, 1:2] = summed

    @pl.when(z == 0)
    def _():
        higher = jnp.maximum(top, own_s[...])
        past, now = jnp.exp(top - higher), jnp.exp(own_s[...] - higher)
        value = jnp.concatenate([value_s[...]] * HEADS, axis=0)
        joined = found * as_column(past, tall_rows) + value * as_column(now, tall_rows)
        bsend[last] = joined.astype(jnp.bfloat16)
        bstat[last, 0:1] = higher
        bstat[last, 1:2] = summed * past + now

    for d in far_first:
        remote(bsend.at[last], bz.at[d - 1], 8, at_z(d)).start()
        remote(bstat.at[last], bsz.at[d - 1], 9, at_z(d)).start()
    arrived(wo_v.at[pl.ds(0, (ny - 1) * columns)], 4)
    arrived(bsz, 9)
    stats = [bstat[last]] + [bsz[d] for d in range(nz - 1)]
    top = functools.reduce(jnp.maximum, [s[0:1] for s in stats])
    factors = [jnp.exp(s[0:1] - top) for s in stats]
    summed = functools.reduce(jnp.add, [s[1:2] * f for s, f in zip(stats, factors)])
    shares = [as_column(f / summed, tall_rows) for f in factors]
    arrived(bz, 8)
    found = bsend[last].astype(jnp.float32) * shares[0]
    for d in range(nz - 1):
        found = found + bz[d].astype(jnp.float32) * shares[d + 1]

    found = found.astype(jnp.bfloat16)
    wide = jnp.concatenate([found[n * ROWS : (n + 1) * ROWS] for n in range(HEADS)], axis=1)
    total = lax.dot_general(wide, wo_v[...], (((1,), (1,)), ((), ())), preferred_element_type=jnp.float32)
    pairs = ny // 2
    for k in range(pairs):
        ots[k] = total[:, k * HEAD_DIM : (k + 1) * HEAD_DIM].astype(jnp.bfloat16)

    pl.semaphore_wait(here.at[3], ntp - 1)
    to = [(dy, dt) for dy in range(ny) for dt in range(ntp) if (dy, dt) != (0, 0)]
    for dy, dt in sorted(to, key=lambda t: -min(t[0], ny - t[0]) - min(t[1] // 2, ntp // 2 - t[1] // 2)):
        there = turned(y, dy, ny)
        remote(ots.at[there // 2], ot.at[dt * ny + dy], 10, (z * ny + there, turned(tp, dt, ntp))).start()
    ot[0] = ots[y // 2]
    arrived(ot.at[pl.ds(1, ntp * ny - 1)], 10)
    odd = lax.rem(y, 2) == 1
    for dy in range(ny):
        total = ot[dy].astype(jnp.float32)
        for dt in range(1, ntp):
            total = total + ot[dt * ny + dy].astype(jnp.float32)
        total = jnp.where(odd, pltpu.roll(total, HEAD_DIM // 2, 1), total)
        out[pl.ds(pl.multiple_of(turned(y, ny - dy, ny) * ROWS, ROWS), ROWS)] = total

    left(ry, 0)
    left(qz, 1)
    left(sqz, 2)
    @pl.when(z != 0)
    def _():
        left(acc.at[4:7], 3)
    left(wo_v.at[pl.ds(0, (ny - 1) * columns)], 4)
    left(q_all.at[pl.ds(0, HEADS * ny - 1)], 5)
    left(by, 6)
    left(bys, 7)
    left(bz, 8)
    left(bsz, 9)
    left(ot.at[pl.ds(1, ntp * ny - 1)], 10)


def local(
    nz, ny, ntp,
    tokens, norm_gain, w_query, w_key, w_value, w_forget, forget_bias, key_cache, value_cache, gate_cache, lengths, w_out,
):
    f32, bf16 = jnp.float32, jnp.bfloat16
    rows, span = key_cache.shape[0], key_cache.shape[1]
    wide, columns = HEAD_DIM * HEADS, w_out.shape[1]
    args = (
        tokens, norm_gain.reshape(1, -1), w_query, w_key, w_value, w_forget.T, forget_bias,
        key_cache, value_cache, gate_cache, lengths, w_out.T,
    )
    own = tokens.shape[1]
    scratch = [
        pltpu.VMEM((rows, own), bf16), pltpu.VMEM((1, own), bf16), pltpu.VMEM((own, wide), bf16),
        pltpu.VMEM((own, HEAD_DIM), bf16), pltpu.VMEM((own, HEAD_DIM), bf16), pltpu.VMEM((HEADS, own), bf16),
        pltpu.VMEM((ny * columns, wide), bf16), pltpu.VMEM((rows, span, HEAD_DIM), bf16), pltpu.VMEM((rows, span, HEAD_DIM), bf16),
        pltpu.VMEM((rows, HEADS, span), f32), pltpu.SMEM((HEADS,), f32), pltpu.SMEM((rows,), jnp.int32),
        pltpu.VMEM((ny, 7, ROWS, HEAD_DIM), f32),
        pltpu.VMEM((ny - 1, 7, ROWS, HEAD_DIM), f32),
        pltpu.VMEM((7, ROWS, HEAD_DIM), f32),
        pltpu.VMEM((1, HEAD_DIM), f32),
        pltpu.VMEM((nz - 1, ROWS, HEAD_DIM), f32),
        pltpu.VMEM((nz - 1, 1, HEAD_DIM), f32),
        pltpu.VMEM((nz - 1, 3, ROWS, HEAD_DIM), f32),
        pltpu.VMEM((ny * HEADS, ROWS, HEAD_DIM), bf16),
        pltpu.VMEM((ny, HEADS * ROWS, span), f32),
        pltpu.VMEM((ny, HEADS * ROWS, HEAD_DIM), bf16),
        pltpu.VMEM((ny, 2, HEAD_DIM), f32),
        pltpu.VMEM((ny - 1, HEADS * ROWS, HEAD_DIM), bf16),
        pltpu.VMEM((ny - 1, 2, HEAD_DIM), f32),
        pltpu.VMEM((nz - 1, HEADS * ROWS, HEAD_DIM), bf16),
        pltpu.VMEM((nz - 1, 2, HEAD_DIM), f32),
        pltpu.VMEM((1, HEAD_DIM), f32),
        pltpu.VMEM((ROWS, HEAD_DIM), f32),
        pltpu.VMEM((ny // 2, ROWS, HEAD_DIM), bf16),
        pltpu.VMEM((ntp * ny, ROWS, HEAD_DIM), bf16),
        pltpu.SemaphoreType.DMA((12,)),
        pltpu.SemaphoreType.DMA((11,)), pltpu.SemaphoreType.DMA((11,)), pltpu.SemaphoreType.REGULAR((4,)),
    ]
    mixed = pl.pallas_call(
        functools.partial(kernel, nz, ny, ntp),
        out_shape=pltpu.VMEM((rows, HEAD_DIM), f32),
        in_specs=[pl.BlockSpec(memory_space=pl.ANY)] * 12,
        out_specs=pl.BlockSpec(memory_space=pltpu.VMEM),
        scratch_shapes=scratch,
        compiler_params=pltpu.CompilerParams(collective_id=0, has_side_effects=True),
        name="step",
    )(*args)
    return mixed[:, :columns].astype(bf16)


def solution(mesh):
    ny, ntp = NY, mesh.shape["tp"]
    nz = mesh.shape["kv"] // ny
    return jax.shard_map(
        functools.partial(local, nz, ny, ntp),
        mesh=mesh,
        in_specs=(
            P(None, "kv"), P("kv"), P("kv", "tp"), P("kv", "tp"), P("kv", "tp"), P("kv", "tp"), P("tp"),
            P(None, "kv", "tp"), P(None, "kv", "tp"), P(None, "tp", "kv"), P(), P("tp", "kv"),
        ),
        out_specs=P(None, "kv"),
        check_vma=False,
    )
```

time: 57.5 us -> 52.1 us (0.906)
  Pallas kernels: 55.9 us -> 51.3 us
  local copies, waits for them, and re-layouts: 1.3 us -> 0.6 us
    pallas_call x1, Pallas kernels: 55.9 us -> 51.3 us  [local(): pl.pallas_call(functools.partial(kernel, nz, ny, ntp), out_shape=pltpu.VM...]
    unnamed x1 -> x0, local copies, waits for them, and re-layouts: 1.3 us -> none
    slice x0 -> x1, local copies, waits for them, and re-layouts: none -> 0.6 us  [local(): return mixed[:, :columns].astype(bf16)]
where the time goes in v2:
time: 52.1 us; the launch traced here: 51.9 us
  Pallas kernels  51.3 us (98%)
  local copies, waits for them, and re-layouts  0.6 us (1%)
    pallas_call x1, Pallas kernels, local(): pl.pallas_call(functools.partial(kernel, nz, ny, ntp), out_shape=pltpu.VM...  51.3 us

profile of v2, /device:TPU:1, one launch (start us, length us, event | category | flops | bytes accessed | tf_op | source)
XLA Modules:
  0.0 51.9 jit_solution(9877907136842005120)
XLA Ops:
  0.0 51.3 %step.1 = f32[32,128]{1,0:T(8,128)S(1)} custom-call(bf16[32,64]{1,0:T(8,128)(2,1)} %tokens.1, bf16[1,64]{1,0:T(2,128)(2,1)} %bitcast.5, bf16[64,512]{1,0:T(8,128)(2,1)} %w_query.1, bf16[64,128]{1,0:T(8,128)(2,1)} %w_key.1, bf16[64,128]{1,0:T(8,128)(2,1)} %w_value.1, bf16[4,64]{1,0:T(4,128)(2,1)} %bitcast.4, f32[4]{0:T(128)} %bias.1, ...), custom_call_target="tpu_custom_call" | custom-call | tf_op jit(solution)/shard_map/step/pallas_call | solution.py:356
  51.3 0.6 %slice.7 = bf16[32,64]{1,0:T(8,128)(2,1)} slice(f32[32,128]{1,0:T(8,128)S(1)} %step.1), slice={[0:32], [0:64]} | slice | bytes 8192 | tf_op jit(solution)/shard_map/slice | solution.py:365

commit v3 on v2

--- a/solution.py
+++ b/solution.py
@@ -22,7 +22,7 @@
     tokens, gain, w_query, w_key, w_value, w_forget, bias, keys, values, gates, lengths, w_out,
     out,
     tok_v, gain_v, wq_v, wk_v, wv_v, wf_v, wo_v, k_v, v_v, g_v, bias_s, len_s,
-    part, ry, acc, sqrow, qz, sqz, kvz, q_all, gp,
+    kt, part, ry, rykv, acc, sqrow, qz, sqz, kvz, q_all, gp,
     bsend, bstat, by, bys, bz, bsz, own_s, value_s, ots, ot,
     in_sem, send, recv, here,
 ):
@@ -56,34 +56,29 @@
     for c in loads:
         c.start()
 
-    half = nz // 2
-
-    def rank_of(i):
-        return i if i < half else nz - 1 + half - i
-
-    rank = jnp.where(z < half, z, nz - 1 + half - z)
     barrier = pltpu.get_barrier_semaphore()
-    meetings = (
-        [(rank, rank_of(i), (i * ny + y, tp), 0) for i in sorted(range(nz), key=rank_of, reverse=True)]
-        + [(y, i, (z * ny + i, tp), 1) for i in range(ny)]
-        + [(tp, i, (kv, i), 2) for i in range(ntp)]
-    )
-    for me, other, peer, _ in meetings:
-        @pl.when(me < other)
-        def _(peer=peer):
-            pl.semaphore_signal(barrier, inc=1, device_id=peer, device_id_type=MESH)
-    earlier = rank + y + tp
-
-    @pl.when(earlier > 0)
-    def _():
-        pl.semaphore_wait(barrier, earlier)
-
-    for kind in range(3):
-        pl.semaphore_signal(here.at[kind], inc=1)
-    for me, other, peer, kind in meetings:
-        @pl.when(me > other)
-        def _(peer=peer, kind=kind):
-            pl.semaphore_signal(here.at[kind], inc=1, device_id=peer, device_id_type=MESH)
+    close = sorted({d % nz for d in (2, -2, 1, -1)}, key=lambda d: -min(d, nz - d))
+    greeted = [at_z(d) for d in close] + [at_y(d) for d in range(1, ny)]
+    for peer in greeted:
+        pl.semaphore_signal(barrier, inc=1, device_id=peer, device_id_type=MESH)
+    for i in range(ntp):
+        @pl.when(tp < i)
+        def _(i=i):
+            pl.semaphore_signal(barrier, inc=1, device_id=(kv, i), device_id_type=MESH)
+    pl.semaphore_wait(barrier, len(greeted) + tp)
+    strides = [d for d in (2, 4) if 2 * d <= nz // 2]
+
+    def tell(step):
+        for d in (strides[step], nz - strides[step]):
+            pl.semaphore_signal(here.at[step], inc=1, device_id=at_z(d), device_id_type=MESH)
+
+    if strides:
+        tell(0)
+    pl.semaphore_signal(here.at[2], inc=1)
+    for i in range(ntp):
+        @pl.when(tp > i)
+        def _(i=i):
+            pl.semaphore_signal(here.at[2], inc=1, device_id=(kv, i), device_id_type=MESH)
 
     def remote(src, dst, phase, peer):
         return pltpu.make_async_remote_copy(
@@ -119,7 +114,7 @@
         p = jnp.dot(scaled, wq_v[:, t * HEAD_DIM : (t + 1) * HEAD_DIM], preferred_element_type=jnp.float32)
         for j in range(ny):
             part[j, t] = p[j * ROWS : (j + 1) * ROWS]
-    for t, w in ((4, wk_v), (5, wv_v)):
+    for t, w in ((5, wk_v), (6, wv_v)):
         p = jnp.dot(scaled, w[...], preferred_element_type=jnp.float32)
         for j in range(ny):
             part[j, t] = p[j * ROWS : (j + 1) * ROWS]
@@ -129,11 +124,15 @@
         for n in range(HEADS):
             f = jnp.broadcast_to(p[j * ROWS : (j + 1) * ROWS, n : n + 1], (ROWS, HEAD_DIM))
             side = jnp.where(lane == n, f, side)
-        part[j, 6] = side
-
-    pl.semaphore_wait(here.at[1], ny - y)
+        part[j, 4] = side
+
     for d in range(1, ny):
-        remote(part.at[turned(y, d, ny)], ry.at[d - 1], 0, at_y(d)).start()
+        remote(part.at[turned(y, d, ny), 0:5], ry.at[d - 1], 0, at_y(d)).start()
+    for d in range(1, ny):
+        remote(part.at[turned(y, d, ny), 5:7], rykv.at[d - 1], 11, at_y(d)).start()
+    for step in range(1, len(strides)):
+        pl.semaphore_wait(here.at[step - 1], 2)
+        tell(step)
 
     loads[6].wait()
     loads[7].wait()
@@ -146,19 +145,26 @@
                 gp[j, n * ROWS + i : n * ROWS + i + 1, :] = jnp.where(valid, g_v[b, n : n + 1, :], NEGATIVE)
 
     arrived(ry, 0)
-    for t in range(7):
+    for t in range(5):
         total = part[y, t]
         for d in range(ny - 1):
             total = total + ry[d, t]
         acc[t] = total
-    sqrow[...] = as_row(acc[6][:, HEADS : HEADS + 1])
-
-    pl.semaphore_wait(here.at[0], nz - rank)
+    sqrow[...] = as_row(acc[4][:, HEADS : HEADS + 1])
+
+    if strides:
+        pl.semaphore_wait(here.at[len(strides) - 1], 2)
     far_first = sorted(range(1, nz), key=lambda d: -min(d, nz - d))
     for d in far_first:
         remote(acc.at[lax.rem(turned(z, d, nz), HEADS)], qz.at[d - 1], 1, at_z(d)).start()
         remote(sqrow, sqz.at[d - 1], 2, at_z(d)).start()
 
+    arrived(rykv, 11)
+    for t in range(2):
+        total = part[y, 5 + t]
+        for d in range(ny - 1):
+            total = total + rykv[d, t]
+        acc[5 + t] = total
     for d in range(1, nz):
         @pl.when(z == d)
         def _(d=d):
@@ -171,6 +177,15 @@
     pl.semaphore_wait(here.at[2], ntp - tp)
     for d in range(1, ntp):
         pl.semaphore_signal(here.at[3], inc=1, device_id=(kv, turned(tp, d, ntp)), device_id_type=MESH)
+    pl.semaphore_signal(here.at[3], inc=1)
+
+    loads[9].wait()
+
+    def turn(b, carry):
+        kt[b] = k_v[b].T
+        return carry
+
+    lax.fori_loop(0, k_v.shape[0], turn, 0, unroll=4)
 
     arrived(sqz, 2)
     line = sqrow[...]
@@ -187,19 +202,22 @@
     for dz, dy in sorted(near, key=lambda t: -abs(t[0]) - min(t[1], ny - t[1])):
         peer = (turned(z, dz % nz, nz) * ny + turned(y, dy, ny), tp)
         remote(q_all.at[slot], q_all.at[slot], 5, peer).start()
-    loads[9].wait()
     loads[10].wait()
     arrived(q_all.at[pl.ds(0, HEADS * ny - 1)], 5)
 
     tall = lax.rem(lax.broadcasted_iota(jnp.int32, (tall_rows, 1), 0), ROWS)
-    for d in tuple(range(ny // 2, ny)) + tuple(range(1, ny // 2)) + (0,):
+    wanted = sorted(range(1, ny), key=lambda d: -min(d, ny - d))
+
+    def score(d):
         j = turned(y, d, ny)
         q = jnp.concatenate([q_all[j * HEADS + n] for n in range(HEADS)], axis=0)
         scores = jnp.zeros((tall_rows, span), jnp.float32)
         for i in range(ROWS):
-            s = lax.dot_general(q, k_v[j * ROWS + i], (((1,), (1,)), ((), ())), preferred_element_type=jnp.float32)
-            scores = jnp.where(tall == i, s, scores)
-        scores = scores * scaling + gp[j]
+            scores = jnp.where(tall == i, jnp.dot(q, kt[j * ROWS + i], preferred_element_type=jnp.float32), scores)
+        return scores * scaling + gp[j]
+
+    def weigh(d, scores):
+        j = turned(y, d, ny)
         top = jnp.max(scores, axis=1, keepdims=True)
         weights = jnp.exp(scores - top)
         summed = jnp.sum(weights, axis=1, keepdims=True)
@@ -207,13 +225,24 @@
         for i in range(ROWS):
             w = jnp.where(tall == i, weights, 0.0).astype(jnp.bfloat16)
             found = found + jnp.dot(w, v_v[j * ROWS + i], preferred_element_type=jnp.float32)
-        top, summed = as_row(top), as_row(summed)
-        if d:
-            bsend[d - 1] = found.astype(jnp.bfloat16)
-            bstat[d - 1, 0:1] = top
-            bstat[d - 1, 1:2] = summed
-            remote(bsend.at[d - 1], by.at[d - 1], 6, at_y(d)).start()
-            remote(bstat.at[d - 1], bys.at[d - 1], 7, at_y(d)).start()
+        return found, as_row(top), as_row(summed)
+
+    def post(d, found, top, summed):
+        bsend[d - 1] = found.astype(jnp.bfloat16)
+        bstat[d - 1, 0:1] = top
+        bstat[d - 1, 1:2] = summed
+
+    def hand(d):
+        remote(bsend.at[d - 1], by.at[d - 1], 6, at_y(d)).start()
+        remote(bstat.at[d - 1], bys.at[d - 1], 7, at_y(d)).start()
+
+    scores = {d: score(d) for d in wanted}
+    for some in (wanted[:1], wanted[1:]):
+        for d in some:
+            post(d, *weigh(d, scores[d]))
+        for d in some:
+            hand(d)
+    found, top, summed = weigh(0, score(0))
 
     @pl.when(z == 0)
     def _():
@@ -222,11 +251,11 @@
         new = [acc[4 + t] for t in range(3)]
         for d in range(nz - 1):
             new = [new[t] + kvz[d, t] for t in range(3)]
-        new_key = (new[0] * rate).astype(jnp.bfloat16).astype(jnp.float32)
-        value_s[...] = (new[1] * rate).astype(jnp.bfloat16).astype(jnp.float32)
+        new_key = (new[1] * rate).astype(jnp.bfloat16).astype(jnp.float32)
+        value_s[...] = (new[2] * rate).astype(jnp.bfloat16).astype(jnp.float32)
         own = []
         for n in range(HEADS):
-            forget = new[2][:, n : n + 1] * rate + bias_s[n]
+            forget = new[0][:, n : n + 1] * rate + bias_s[n]
             log_forget = jnp.minimum(forget, 0.0) - jnp.log1p(jnp.exp(-jnp.abs(forget)))
             query = q_all[y * HEADS + n].astype(jnp.float32)
             own.append(jnp.sum(query * new_key, axis=1, keepdims=True) * scaling - log_forget)
@@ -284,7 +313,7 @@
     for k in range(pairs):
         ots[k] = total[:, k * HEAD_DIM : (k + 1) * HEAD_DIM].astype(jnp.bfloat16)
 
-    pl.semaphore_wait(here.at[3], ntp - 1)
+    pl.semaphore_wait(here.at[3], ntp)
     to = [(dy, dt) for dy in range(ny) for dt in range(ntp) if (dy, dt) != (0, 0)]
     for dy, dt in sorted(to, key=lambda t: -min(t[0], ny - t[0]) - min(t[1] // 2, ntp // 2 - t[1] // 2)):
         there = turned(y, dy, ny)
@@ -300,6 +329,7 @@
         out[pl.ds(pl.multiple_of(turned(y, ny - dy, ny) * ROWS, ROWS), ROWS)] = total
 
     left(ry, 0)
+    left(rykv, 11)
     left(qz, 1)
     left(sqz, 2)
     @pl.when(z != 0)
@@ -331,8 +361,10 @@
         pltpu.VMEM((own, HEAD_DIM), bf16), pltpu.VMEM((own, HEAD_DIM), bf16), pltpu.VMEM((HEADS, own), bf16),
         pltpu.VMEM((ny * columns, wide), bf16), pltpu.VMEM((rows, span, HEAD_DIM), bf16), pltpu.VMEM((rows, span, HEAD_DIM), bf16),
         pltpu.VMEM((rows, HEADS, span), f32), pltpu.SMEM((HEADS,), f32), pltpu.SMEM((rows,), jnp.int32),
+        pltpu.VMEM((rows, HEAD_DIM, span), bf16),
         pltpu.VMEM((ny, 7, ROWS, HEAD_DIM), f32),
-        pltpu.VMEM((ny - 1, 7, ROWS, HEAD_DIM), f32),
+        pltpu.VMEM((ny - 1, 5, ROWS, HEAD_DIM), f32),
+        pltpu.VMEM((ny - 1, 2, ROWS, HEAD_DIM), f32),
         pltpu.VMEM((7, ROWS, HEAD_DIM), f32),
         pltpu.VMEM((1, HEAD_DIM), f32),
         pltpu.VMEM((nz - 1, ROWS, HEAD_DIM), f32),
@@ -351,7 +383,7 @@
         pltpu.VMEM((ny // 2, ROWS, HEAD_DIM), bf16),
         pltpu.VMEM((ntp * ny, ROWS, HEAD_DIM), bf16),
         pltpu.SemaphoreType.DMA((12,)),
-        pltpu.SemaphoreType.DMA((11,)), pltpu.SemaphoreType.DMA((11,)), pltpu.SemaphoreType.REGULAR((4,)),
+        pltpu.SemaphoreType.DMA((12,)), pltpu.SemaphoreType.DMA((12,)), pltpu.SemaphoreType.REGULAR((4,)),
     ]
     mixed = pl.pallas_call(
         functools.partial(kernel, nz, ny, ntp),

time: 52.1 us -> 49.8 us (0.956)
  Pallas kernels: 51.3 us -> 49.1 us
    pallas_call x1, Pallas kernels: 51.3 us -> 49.1 us  [local(): pl.pallas_call(functools.partial(kernel, nz, ny, ntp), out_shape=pltpu.VM...]
where the time goes in v3:
time: 49.8 us; the launch traced here: 49.7 us
  Pallas kernels  49.1 us (99%)
  local copies, waits for them, and re-layouts  0.6 us (1%)
    pallas_call x1, Pallas kernels, local(): pl.pallas_call(functools.partial(kernel, nz, ny, ntp), out_shape=pltpu.VM...  49.1 us

profile of v3, /device:TPU:1, one launch (start us, length us, event | category | flops | bytes accessed | tf_op | source)
XLA Modules:
  0.0 49.7 jit_solution(7781764717751292713)
XLA Ops:
  0.0 49.1 %step.1 = f32[32,128]{1,0:T(8,128)S(1)} custom-call(bf16[32,64]{1,0:T(8,128)(2,1)} %tokens.1, bf16[1,64]{1,0:T(2,128)(2,1)} %bitcast.5, bf16[64,512]{1,0:T(8,128)(2,1)} %w_query.1, bf16[64,128]{1,0:T(8,128)(2,1)} %w_key.1, bf16[64,128]{1,0:T(8,128)(2,1)} %w_value.1, bf16[4,64]{1,0:T(4,128)(2,1)} %bitcast.4, f32[4]{0:T(128)} %bias.1, ...), custom_call_target="tpu_custom_call" | custom-call | tf_op jit(solution)/shard_map/step/pallas_call | solution.py:388
  49.1 0.6 %slice.7 = bf16[32,64]{1,0:T(8,128)(2,1)} slice(f32[32,128]{1,0:T(8,128)S(1)} %step.1), slice={[0:32], [0:64]} | slice | bytes 8192 | tf_op jit(solution)/shard_map/slice | solution.py:397
